TPU v7x, 32 devices: a whole 2x2x4 slice. The times are simulated.
32 devices in a mesh: fs: 8 (over z, x), tp: 4 (over y, core).
Axes of the slice: x: 2, y: 2, z: 4, core: 2. Of those that a mesh axis runs over, the one named last changes fastest.
Arguments:
- inputs: bfloat16 [3072, 2048], P('fs'), may hold values from -6 to 6
- queries: bfloat16 [3072, 2048], P('fs', 'tp'), may hold values from -6 to 6
- keys: bfloat16 [3072, 2048], P('fs', 'tp'), may hold values from -6 to 6
- values: bfloat16 [3072, 2048], P('fs', 'tp'), may hold values from -6 to 6
- head_cot: bfloat16 [3072, 2048], P('fs', 'tp'), may hold values from -6 to 6
- mixing: float32 [16], P('tp'), may hold values from 0.3 to 0.8
- head_gain: float32 [128], replicated, may hold values from 0.1 to 1.9
- factors: bfloat16 [2048, 2, 256], P('fs'), may hold values from -0.375 to 0.375
- moments: float32 [256, 2, 2048], P('fs', None, 'tp'), may hold values from -6 to 6
- weights: float32 [2048, 2, 2048], P('fs', None, 'tp'), may hold values from -6 to 6
Outputs:
- step: float32 [2048, 2, 2048], P('fs', None, 'tp')
- new_moments: float32 [256, 2, 2048], P('fs', None, 'tp')
- copies: bfloat16 [2048, 2, 2048], P(None, None, 'tp')
All inputs are finite; a program needn't handle non-finite values.
Results may differ from a plain program's by a relative error of at most 0.007.
Values may be sent and summed in bfloat16 or wider, within the bound.
A program may use at most 64 MiB of HBM per device.

v0:
```python
import jax
import jax.numpy as jnp
from jax import lax
from jax.sharding import PartitionSpec as P

EPS = 0.05
BETA = 0.9
RATE_BASE = 0.5


def softmax_rows(scores):
    top = jnp.max(scores, axis=-1, keepdims=True)
    expo = jnp.exp(scores - top)
    return expo / jnp.sum(expo, axis=-1, keepdims=True)


def head_grads(query, key_rows, value, upstream, weight_mix, head_gain):
    length = query.shape[0]
    head_dim = query.shape[2]
    factor = head_dim ** (-0.5)
    places = jnp.arange(length)
    causal = places[None, :] <= places[:, None]

    def probs(which):
        scores = (
            jnp.dot(query[:, which], key_rows[:, which].T, preferred_element_type=jnp.float32)
            * factor
        )
        return softmax_rows(jnp.where(causal, scores, -jnp.inf))

    first = probs(0)
    second = probs(1)
    mixed = (first - weight_mix * second).astype(jnp.bfloat16)
    output = jnp.dot(mixed, value, preferred_element_type=jnp.float32)
    inverse = lax.rsqrt(jnp.mean(output * output, axis=-1, keepdims=True) + EPS)
    scaled = head_gain * upstream.astype(jnp.float32)
    d_out = inverse * scaled - output * inverse**3 * jnp.mean(
        output * scaled, axis=-1, keepdims=True
    )
    d_out = d_out.astype(jnp.bfloat16)
    d_value = jnp.dot(mixed.T, d_out, preferred_element_type=jnp.float32).astype(jnp.bfloat16)
    d_mix = jnp.dot(d_out, value.T, preferred_element_type=jnp.float32)
    d_first = (first * (d_mix - jnp.sum(first * d_mix, axis=-1, keepdims=True))).astype(
        jnp.bfloat16
    )
    d_second = (
        -weight_mix * second * (d_mix - jnp.sum(second * d_mix, axis=-1, keepdims=True))
    ).astype(jnp.bfloat16)
    q_first = (
        jnp.dot(d_first, key_rows[:, 0], preferred_element_type=jnp.float32) * factor
    ).astype(jnp.bfloat16)
    q_second = (
        jnp.dot(d_second, key_rows[:, 1], preferred_element_type=jnp.float32) * factor
    ).astype(jnp.bfloat16)
    return (jnp.stack([q_first, q_second], axis=1).reshape(length, 2 * head_dim), d_value)


def per_device(
    inputs, queries, keys, values, head_cot, mixing, head_gain, factors, moments, weights
):
    length = inputs.shape[0]
    heads_here = mixing.shape[0]
    head_width = values.shape[1] // heads_here
    head_dim = head_width // 2
    query_heads = queries.reshape(length, heads_here, 2, head_dim).transpose(1, 0, 2, 3)
    key_heads = keys.reshape(length, heads_here, 2, head_dim).transpose(1, 0, 2, 3)
    value_heads = values.reshape(length, heads_here, head_width).transpose(1, 0, 2)
    upstream_heads = head_cot.reshape(length, heads_here, head_width).transpose(1, 0, 2)

    def one_head(pieces):
        return head_grads(pieces[0], pieces[1], pieces[2], pieces[3], pieces[4], head_gain)

    d_query, d_value = lax.map(
        one_head, (query_heads, key_heads, value_heads, upstream_heads, mixing)
    )
    d_query = d_query.transpose(1, 0, 2).reshape(length, heads_here * head_width)
    d_value = d_value.transpose(1, 0, 2).reshape(length, heads_here * head_width)
    cotangents = jnp.stack([d_query, d_value], axis=1)
    fs_count = lax.axis_size("fs")
    token_factor = (length * fs_count) ** (-0.5)
    rank_here = moments.shape[0]
    cols_here = moments.shape[2]
    factor_wide = factors.astype(jnp.float32)
    whole_factors = lax.all_gather(factors, "fs", axis=0, tiled=True)
    reduced = jnp.einsum("td,dkr->tkr", inputs, whole_factors, preferred_element_type=jnp.float32)
    reduced_upper = reduced.astype(jnp.bfloat16)
    reduced_lower = (reduced - reduced_upper.astype(jnp.float32)).astype(jnp.bfloat16)
    upper_part = jnp.einsum(
        "tkr,tke->rke", reduced_upper, cotangents, preferred_element_type=jnp.float32
    )
    lower_part = jnp.einsum(
        "tkr,tke->rke", reduced_lower, cotangents, preferred_element_type=jnp.float32
    )
    projected = lax.psum_scatter(upper_part + lower_part, "fs", scatter_dimension=0, tiled=True)
    projected = projected * token_factor
    new_moments = BETA * moments + projected
    local_sums = jnp.sum(new_moments * new_moments, axis=(0, 2))
    totals = lax.psum(local_sums, ("fs", "tp"))
    entries = rank_here * fs_count * cols_here * lax.axis_size("tp")
    rate = RATE_BASE / jnp.sqrt(1.0 + totals / entries)
    low_part = jnp.einsum(
        "dkr,rke->dke",
        factor_wide,
        lax.all_gather(new_moments, "fs", axis=0, tiled=True),
        precision=lax.Precision.HIGHEST,
    )
    step = low_part * rate[None, :, None]
    copies = lax.all_gather((weights - step).astype(jnp.bfloat16), "fs", axis=0, tiled=True)
    return (step, new_moments, copies)


def solution(mesh):
    placed = (
        P("fs", None),
        P("fs", "tp"),
        P("fs", "tp"),
        P("fs", "tp"),
        P("fs", "tp"),
        P("tp"),
        P(),
        P("fs", None, None),
        P("fs", None, "tp"),
        P("fs", None, "tp"),
    )
    return jax.shard_map(
        per_device,
        mesh=mesh,
        in_specs=placed,
        out_specs=(P("fs", None, "tp"), P("fs", None, "tp"), P(None, None, "tp")),
        check_vma=False,
    )
```

profile of v0, /device:TPU:0, one launch (start us, length us, event | category | flops | bytes accessed | tf_op | source)
XLA Modules:
  0.0 282.7 jit_solution(10454785109164463003)
XLA Ops:
  7.3 1.8 copy.46
  9.2 1.2 copy.39
  10.4 1.2 copy.40
  11.8 1.2 copy.42
  13.0 21.3 %while.12 = (s32[]{:T(128)}, bf16[4,384,128]{1,2,0:T(8,128)(2,1)S(1)}, bf16[4,384,128]{2,1,0:T(8,128)(2,1)}, bf16[4,384,2,64]{1,3,2,0:T(8,128)(2,1)S(1)}, bf16[4...) while((s32[]{:T(128)}, ...), condition=%wide.region_9.10_spmd, body=%wide.region_0.9_spmd.sunk | while | flops 195525504 | bytes 10978449 | solution.py:73
  16.3 1.0 fusion.71
  20.5 0.8 subtract_convert_fusion.5
  21.6 1.0 fusion.71
  25.8 0.8 subtract_convert_fusion.5
  26.9 1.0 fusion.71
  31.2 0.8 subtract_convert_fusion.5
  32.3 1.0 fusion.71
  34.3 1.2 copy.45
  35.6 27.0 %all-gather.4.cloned.1.call-done = bf16[2048,2,256]{2,0,1:T(8,128)(2,1)} async-done(((bf16[256,2,256]{2,0,1:T(8,128)(2,1)}), bf16[2048,2,256]{2,0,1:T(8,128)(2,1)}) %all-gather.4.cloned.1.call-update) | async-done | bytes 2097168 | tf_op jit(solution)/shard_map/all_gather | solution.py:84
  62.6 2.6 fusion.30
  66.1 1.3 copy.47
  68.7 75.5 %all-reduce.3.cloned.1.call-done = f32[256,2,512]{2,1,0:T(2,128)} async-done(((f32[256,2,512]{2,1,0:T(2,128)}), f32[256,2,512]{2,1,0:T(2,128)}) %all-reduce.3.cloned.1.call-update) | async-done | bytes 1048592
  144.3 1.8 multiply_reduce_fusion.3
  146.1 1.4 copy.50
  147.6 39.7 %psum.7 = f32[2]{0:T(128)S(1)} all-reduce(f32[2]{0:T(128)S(1)} %get-tuple-element.111), channel_id=1, replica_groups=mesh['fs'=8,'tp'=4] {'fs','tp'}, use_global_device_ids=true, to_apply=%region_12.13 | all-reduce | flops 2 | bytes 16 | tf_op jit(solution)/shard_map/psum | solution.py:98
  187.3 3.5 %subtract_convert_fusion.1 = (bf16[256,2,512]{0,2,1:T(8,128)(2,1)}, f32[256,2,512]{0,2,1:T(8,128)S(1)}) fusion(f32[256,2,512]{0,2,1:T(8,128)} %copy.50, f32[2]{0:T(128)S(1)} %rsqrt_multiply_fusion, bf16[256,2,256]{2,1,0:T(2,128)(2,1)S(1)} %copy-done.1, f32[256,2,512]{2,1,0:T(2,128)} %all-gather.6.cloned.1.call-done), kind=kOutput, calls=%fused_computation.61 | convolution fusion | flops 806092800 | bytes 3932168 | tf_op jit(solution)/shard_map/dkr,rke->dke/dot_general | solution.py:101
  190.8 1.3 copy.51
  192.1 72.9 %all-gather.8.cloned.1.call-done = bf16[2048,2,512]{0,2,1:T(8,128)(2,1)} async-done(((bf16[256,2,512]{0,2,1:T(8,128)(2,1)}), bf16[2048,2,512]{0,2,1:T(8,128)(2,1)}) %all-gather.8.cloned.1.call-update) | async-done | bytes 4194320 | tf_op jit(solution)/shard_map/all_gather | solution.py:108
  265.0 11.1 %copy.52 = bf16[2048,2,512]{2,1,0:T(2,128)(2,1)} copy(bf16[2048,2,512]{0,2,1:T(8,128)(2,1)} %all-gather.8.cloned.1.call-done) | data formatting | bytes 8388608
  (89 shorter events, 14.0 us)
Async XLA Ops:
  7.2 55.4 %copy-start = (bf16[384,2048]{1,0:T(8,128)(2,1)S(1)}, bf16[384,2048]{1,0:T(8,128)(2,1)}, u32[]{:S(2)}) copy-start(bf16[384,2048]{1,0:T(8,128)(2,1)} %param.12) | copy-start | bytes 4718596
  7.2 4.4 %copy-start.3 = (bf16[384,512]{1,0:T(8,128)(2,1)S(1)}, bf16[384,512]{1,0:T(8,128)(2,1)}, u32[]{:S(2)}) copy-start(bf16[384,512]{1,0:T(8,128)(2,1)} %param.15) | copy-start | bytes 1179652
  7.2 5.8 %copy-start.5 = (f32[128]{0:T(128)S(1)}, f32[128]{0:T(128)}, u32[]{:S(2)}) copy-start(f32[128]{0:T(128)} %param.18) | copy-start | bytes 1540
  7.2 5.8 %copy-start.6 = (f32[4]{0:T(128)S(1)}, f32[4]{0:T(128)}, u32[]{:S(2)}) copy-start(f32[4]{0:T(128)} %param.17) | copy-start | bytes 52
  7.2 55.4 %all-gather.4.cloned.1.call-start = ((), (), s32[]{:S(2)}) async-start(), calls=%async_computation | async-start | bytes 2359296 | tf_op jit(solution)/shard_map/all_gather | solution.py:84
  9.1 135.2 %all-reduce.3.cloned.1.call-start = ((), (), s32[]{:S(2)}) async-start(), calls=%async_computation.3 | async-start | bytes 2097152
  66.1 1.4 copy-start.7
  66.1 78.2 %copy-start.4 = (f32[32,2,512]{2,1,0:T(2,128)S(1)}, f32[32,2,512]{2,1,0:T(2,128)}, u32[]{:S(2)}) copy-start(f32[32,2,512]{2,1,0:T(2,128)} %param.20) | copy-start | bytes 393220
  67.4 78.8 %copy-start.2 = (f32[256,2,512]{2,1,0:T(2,128)S(1)}, f32[256,2,512]{2,1,0:T(2,128)}, u32[]{:S(2)}) copy-start(f32[256,2,512]{2,1,0:T(2,128)} %param.21) | copy-start | bytes 3145732
  67.4 119.9 %copy-start.1 = (bf16[256,2,256]{2,1,0:T(2,128)(2,1)S(1)}, bf16[256,2,256]{2,1,0:T(2,128)(2,1)}, u32[]{:S(2)}) copy-start(bf16[256,2,256]{2,1,0:T(2,128)(2,1)} %param.19) | copy-start | bytes 786436
  67.4 119.9 %all-gather.6.cloned.1.call-start = ((), (), s32[]{:S(2)}) async-start(), calls=%async_computation.1 | async-start | bytes 1179648 | tf_op jit(solution)/shard_map/all_gather | solution.py:104
  146.1 118.9 %all-gather.8.cloned.1.call-start = ((), (), s32[]{:S(2)}) async-start(), calls=%async_computation.2 | async-start | bytes 4718592 | tf_op jit(solution)/shard_map/all_gather | solution.py:108
Sparse Core Ops, SparseCore 0:
  10.8 51.7 all-gather.3
  67.5 76.6 all-reduce.2
  147.0 40.0 all-gather.5
  190.9 74.0 all-gather.7
where the time goes:
time: 283 us
  waiting for transfers between devices  176 us (62%)
  blocking collectives  39.7 us (14%)
  local copies, waits for them, and re-layouts  25.2 us (9%)
  matrix products  18.3 us (6%)
  between operations  14.6 us (5%)
  other arithmetic  6.28 us (2%)
    unnamed x5, waiting for transfers between devices  75.6 us
    all_gather x1, waiting for transfers between devices, per_device(): lax.all_gather((weights - step).astype(jnp.bfloat16), 'fs', axis=0, tiled...  72.9 us
    psum x1, blocking collectives, per_device(): totals = lax.psum(local_sums, ('fs', 'tp'))  39.7 us
    all_gather x1, waiting for transfers between devices, per_device(): whole_factors = lax.all_gather(factors, 'fs', axis=0, tiled=True)  27 us
    unnamed x25, local copies, waits for them, and re-layouts  20.1 us
  transfers between devices with their start and end apart: 4, of which 3 were waited for; matrix products, arithmetic and copies ran while one was open for 10% of the time, Pallas kernels for 0%

commit v1 on v0

v1 whole, which is shorter than its diff:
```python
import functools

import jax
import jax.numpy as jnp
from jax import lax
from jax.experimental import pallas as pl
from jax.experimental.pallas import tpu as pltpu
from jax.sharding import PartitionSpec as P

EPS = 0.05
BETA = 0.9
RATE_BASE = 0.5
MESH = pl.DeviceIdType.MESH


class Gather:
    def __init__(self, n, own, slot, send, recv):
        me = lax.axis_index("fs")
        self.own, self.slot, self.send, self.recv = own, slot, send, recv
        self.n, self.me, self.places = n, me, n // 2
        self.place, self.parity = me // 2, me % 2
        self.partner = me + 1 - 2 * self.parity
        self.started = []

    def put(self, cond, index, half, way):
        target = (self.me - 2, self.me + 2, self.partner)[way]
        if way == 0:
            cond = jnp.logical_and(cond, self.place > 0)
        elif way == 1:
            cond = jnp.logical_and(cond, self.place < self.places - 1)
        mine = index is self.me

        def make():
            return pltpu.make_async_remote_copy(
                src_ref=self.own(half) if mine else self.slot(index, half),
                dst_ref=self.slot(index, half),
                send_sem=self.send.at[index, half, way],
                recv_sem=self.recv.at[index, half],
                device_id={"fs": target},
                device_id_type=MESH,
            )

        @pl.when(cond)
        def _():
            make().start()

        self.started.append((cond, make))

    def arrive(self, cond, index, half):
        @pl.when(cond)
        def _():
            pltpu.make_async_remote_copy(
                src_ref=self.slot(index, half),
                dst_ref=self.slot(index, half),
                send_sem=self.send.at[index, half, 0],
                recv_sem=self.recv.at[index, half],
                device_id={"fs": self.partner},
                device_id_type=MESH,
            ).wait_recv()

    def begin(self):
        true = self.me >= 0
        for half in (0, 1):
            for way in (2, 0, 1):
                self.put(true, self.me, half, way)

    def turn(self):
        true = self.me >= 0
        self.arrive(true, self.partner, 0)
        for way in (0, 1):
            self.put(true, self.partner, 0, way)

    def step(self, s):
        for way in (1, 0):
            place = self.place - s if way == 1 else self.place + s
            cond = jnp.logical_and(place >= 0, place < self.places)
            same = 2 * place + self.parity
            other = 2 * place + 1 - self.parity
            self.arrive(cond, same, 1)
            self.put(cond, same, 1, 2)
            self.put(cond, same, 1, way)
            self.arrive(cond, same, 0)
            self.put(cond, same, 0, way)
            self.arrive(cond, other, 0)
            self.put(cond, other, 0, way)

    def finish_recv(self):
        true = self.me >= 0
        for place in range(self.places):
            self.arrive(true, 2 * place + 1 - self.parity, 1)

    def finish_send(self):
        for cond, make in self.started:

            @pl.when(cond)
            def _(make=make):
                make().wait_send()


def head_step(head, q_ref, k_ref, v_ref, c_ref, mix_ref, gain_ref, dq_ref, dv_ref):
    length = q_ref.shape[0]
    width = gain_ref.shape[1]
    half = width // 2
    factor = half ** (-0.5)
    cols = slice(head * width, (head + 1) * width)
    query, key, value = q_ref[:, cols], k_ref[:, cols], v_ref[:, cols]
    lane = lax.broadcasted_iota(jnp.int32, (length, width), 1)
    zero = jnp.zeros_like(key)
    key0 = jnp.where(lane < half, key, zero)
    key1 = jnp.where(lane < half, zero, key)
    row = lax.broadcasted_iota(jnp.int32, (length, length), 0)
    col = lax.broadcasted_iota(jnp.int32, (length, length), 1)
    causal = col <= row
    mix = mix_ref[head]
    nt = (((1,), (1,)), ((), ()))
    tn = (((0,), (0,)), ((), ()))

    def probs(rows):
        scores = lax.dot_general(query, rows, nt, preferred_element_type=jnp.float32) * factor
        scores = jnp.where(causal, scores, -jnp.inf)
        expo = jnp.exp(scores - jnp.max(scores, axis=-1, keepdims=True))
        return expo * (1.0 / jnp.sum(expo, axis=-1, keepdims=True))

    first, second = probs(key0), probs(key1)
    mixed = (first - mix * second).astype(jnp.bfloat16)
    output = jnp.dot(mixed, value, preferred_element_type=jnp.float32)
    inverse = lax.rsqrt(jnp.mean(output * output, axis=-1, keepdims=True) + EPS)
    scaled = gain_ref[...] * c_ref[:, cols].astype(jnp.float32)
    d_out = inverse * scaled - output * (inverse * inverse * inverse) * jnp.mean(
        output * scaled, axis=-1, keepdims=True
    )
    d_out = d_out.astype(jnp.bfloat16)
    dv_ref[:, cols] = lax.dot_general(mixed, d_out, tn, preferred_element_type=jnp.float32).astype(jnp.bfloat16)
    d_mix = lax.dot_general(d_out, value, nt, preferred_element_type=jnp.float32)
    d_first = first * (d_mix - jnp.sum(first * d_mix, axis=-1, keepdims=True))
    d_second = -mix * second * (d_mix - jnp.sum(second * d_mix, axis=-1, keepdims=True))
    d_query = jnp.dot(d_first.astype(jnp.bfloat16), key0, preferred_element_type=jnp.float32)
    d_query += jnp.dot(d_second.astype(jnp.bfloat16), key1, preferred_element_type=jnp.float32)
    dq_ref[:, cols] = (d_query * factor).astype(jnp.bfloat16)


def kernel(
    n, tp, heads,
    x_ref, q_ref, k_ref, v_ref, c_ref, mix_ref, gain_ref, f_ref, mom_ref, w_ref,
    fall, wall, nmall, nm_ref, tot_ref,
    dq, dv, psend, precv, sums,
    f_send, f_recv, w_send, w_recv, n_send, n_recv, p_send, p_recv, t_send, t_recv,
):
    me = lax.axis_index("fs")
    mt = lax.axis_index("tp")
    barrier = pltpu.get_barrier_semaphore()
    for hop in range(1, n):
        pl.semaphore_signal(barrier, inc=1, device_id={"fs": (me + hop) % n}, device_id_type=MESH)
    for hop in range(1, tp):
        pl.semaphore_signal(barrier, inc=1, device_id={"tp": (mt + hop) % tp}, device_id_type=MESH)
    pl.semaphore_wait(barrier, n - 1 + tp - 1)

    deep = f_ref.shape[0]
    part = deep // 2
    rank = f_ref.shape[1] // 2
    rank_here = rank // n

    def rows(ref):
        def slot(index, half):
            return ref.at[pl.ds(pl.multiple_of(index * deep + half * part, part), part)]

        return slot

    def own(ref):
        return lambda half: ref.at[pl.ds(half * part, part)]

    gather_f = Gather(n, own(f_ref), rows(fall), f_send, f_recv)
    gather_w = Gather(n, own(w_ref), rows(wall), w_send, w_recv)
    gather_n = Gather(
        n, lambda half: nmall.at[me, half], lambda i, half: nmall.at[i, half], n_send, n_recv
    )
    gather_f.begin()
    gather_w.begin()
    here = pl.ds(pl.multiple_of(me * deep, deep), deep)
    fall[here, :] = f_ref[...]
    wall[here, :] = w_ref[...]
    gather_f.turn()
    done = 1
    for head in range(heads):
        head_step(head, q_ref, k_ref, v_ref, c_ref, mix_ref, gain_ref, dq, dv)
        if done < n // 2:
            gather_f.step(done)
            done += 1
    for s in range(done, n // 2):
        gather_f.step(s)
    gather_w.turn()
    gather_f.finish_recv()
    gather_w.step(1)
    for m, cot in enumerate((dq, dv)):
        reduced = jnp.dot(
            x_ref[...], fall[:, m * rank : (m + 1) * rank], preferred_element_type=jnp.float32
        ).astype(jnp.bfloat16)
        partial = lax.dot_general(
            reduced, cot[...], (((0,), (0,)), ((), ())), preferred_element_type=jnp.float32
        )
        for j in range(n):
            psend[j, m] = partial[j * rank_here : (j + 1) * rank_here].astype(psend.dtype)

    def p_copy(hop):
        peer = (me + hop) % n
        return pltpu.make_async_remote_copy(
            src_ref=psend.at[peer],
            dst_ref=precv.at[hop],
            send_sem=p_send.at[hop],
            recv_sem=p_recv.at[hop],
            device_id={"fs": peer},
            device_id_type=MESH,
        )

    for hop in range(1, n):
        p_copy(hop).start()
    for s in range(2, n // 2 - 1):
        gather_w.step(s)
    total = psend[me].astype(jnp.float32)
    for hop in range(1, n):
        p_copy(hop).wait_recv()
        total += precv[hop].astype(jnp.float32)
    length = x_ref.shape[0]
    moments = BETA * mom_ref[...] + total * (length * n) ** (-0.5)
    nm_ref[...] = moments
    nmall[me] = moments.astype(nmall.dtype)
    gather_n.begin()
    gather_w.step(n // 2 - 1)
    gather_n.turn()
    for s in range(1, n // 2):
        gather_n.step(s)
    gather_n.finish_recv()
    everything = nmall[...].astype(jnp.float32)
    squares = jnp.sum(jnp.sum(everything * everything, axis=0), axis=1)
    sums[0] = jnp.sum(squares, axis=1, keepdims=True) + jnp.zeros((2, 128), jnp.float32)

    def t_copy(hop):
        return pltpu.make_async_remote_copy(
            src_ref=sums.at[0],
            dst_ref=sums.at[hop],
            send_sem=t_send.at[hop],
            recv_sem=t_recv.at[hop],
            device_id={"tp": (mt + hop) % tp},
            device_id_type=MESH,
        )

    for hop in range(1, tp):
        t_copy(hop).start()
    gather_w.finish_recv()
    totals = sums[0]
    for hop in range(1, tp):
        t_copy(hop).wait_recv()
        totals += sums[hop]
    tot_ref[...] = totals
    for hop in range(1, tp):
        t_copy(hop).wait_send()
    for hop in range(1, n):
        p_copy(hop).wait_send()
    for gather in (gather_f, gather_w, gather_n):
        gather.finish_send()


def per_device(
    n, tp, inputs, queries, keys, values, head_cot, mixing, head_gain, factors, moments, weights
):
    length, depth = inputs.shape
    heads = mixing.shape[0]
    deep, _, rank = factors.shape
    rank_here, _, cols = moments.shape
    wire = jnp.bfloat16 if rank_here % 16 == 0 else jnp.float32
    vmem = pl.BlockSpec(memory_space=pltpu.VMEM)
    dma = pltpu.SemaphoreType.DMA
    f_flat = factors.reshape(deep, 2 * rank)
    w_flat = weights.astype(jnp.bfloat16).reshape(deep, 2 * cols)
    mom = moments.transpose(1, 0, 2)
    fall, wall, nmall, nm, totals = pl.pallas_call(
        functools.partial(kernel, n, tp, heads),
        out_shape=(
            jax.ShapeDtypeStruct((depth, 2 * rank), jnp.bfloat16),
            jax.ShapeDtypeStruct((depth, 2 * cols), jnp.bfloat16),
            jax.ShapeDtypeStruct((n, 2, rank_here, cols), wire),
            jax.ShapeDtypeStruct((2, rank_here, cols), jnp.float32),
            jax.ShapeDtypeStruct((2, 128), jnp.float32),
        ),
        in_specs=[vmem] * 5 + [pl.BlockSpec(memory_space=pltpu.SMEM)] + [vmem] * 4,
        out_specs=(vmem,) * 5,
        scratch_shapes=[
            pltpu.VMEM((length, cols), jnp.bfloat16),
            pltpu.VMEM((length, cols), jnp.bfloat16),
            pltpu.VMEM((n, 2, rank_here, cols), wire),
            pltpu.VMEM((n, 2, rank_here, cols), wire),
            pltpu.VMEM((tp, 2, 128), jnp.float32),
            dma((n, 2, 3)), dma((n, 2)),
            dma((n, 2, 3)), dma((n, 2)),
            dma((n, 2, 3)), dma((n, 2)),
            dma((n,)), dma((n,)),
            dma((tp,)), dma((tp,)),
        ],
        compiler_params=pltpu.CompilerParams(
            collective_id=0, has_side_effects=True, vmem_limit_bytes=56 * 1024 * 1024
        ),
    )(inputs, queries, keys, values, head_cot, mixing, head_gain[None, :], f_flat, mom, w_flat)
    rate = RATE_BASE / jnp.sqrt(1.0 + totals[:, 0] / (rank * cols * tp))
    steps, copies = [], []
    for m in range(2):
        block = nmall[:, m].reshape(rank, cols).astype(jnp.bfloat16)
        steps.append(
            jnp.dot(factors[:, m], block, preferred_element_type=jnp.float32) * rate[m]
        )
        low = jnp.dot(
            fall[:, m * rank : (m + 1) * rank], block, preferred_element_type=jnp.float32
        )
        copies.append(
            (wall[:, m * cols : (m + 1) * cols].astype(jnp.float32) - low * rate[m]).astype(
                jnp.bfloat16
            )
        )
    return jnp.stack(steps, axis=1), nm.transpose(1, 0, 2), jnp.stack(copies, axis=1)


def solution(mesh):
    placed = (
        P("fs", None),
        P("fs", "tp"),
        P("fs", "tp"),
        P("fs", "tp"),
        P("fs", "tp"),
        P("tp"),
        P(),
        P("fs", None, None),
        P("fs", None, "tp"),
        P("fs", None, "tp"),
    )
    return jax.shard_map(
        functools.partial(per_device, mesh.shape["fs"], mesh.shape["tp"]),
        mesh=mesh,
        in_specs=placed,
        out_specs=(P("fs", None, "tp"), P("fs", None, "tp"), P(None, None, "tp")),
        check_vma=False,
    )
```

time: 283 us -> 153 us (0.54)
  waiting for transfers between devices: 176 us -> 0 us
  Pallas kernels: 0 us -> 114 us
  blocking collectives: 39.7 us -> 0 us
  between operations: 14.6 us -> 0.74 us
  matrix products: 18.3 us -> 6.45 us
  other arithmetic: 6.28 us -> 3.3 us
    pallas_call x0 -> x1, Pallas kernels: none -> 114 us  [per_device(): pl.pallas_call(functools.partial(kernel, n, tp, heads), out_shape=(jax.Sh...]
    all_gather x3 -> x0, waiting for transfers between devices: 100 us -> none  [the longest x1 72.9 us: per_device(): lax.all_gather((weights - step).astype(jnp.bfloat16), 'fs', axis=0, tiled...]
    unnamed x5 -> x0, waiting for transfers between devices: 75.6 us -> none
    psum x1 -> x0, blocking collectives: 39.7 us -> none  [per_device(): totals = lax.psum(local_sums, ('fs', 'tp'))]
    dot_general x32 -> x4, matrix products: 18.3 us -> 6.45 us  [the longest x2 4.62 us: per_device(): jnp.dot(fall[:, m * rank:(m + 1) * rank], block, preferred_element_type=j...]
    unnamed x25 -> x14, local copies, waits for them, and re-layouts: 20.1 us -> 25.4 us
  transfers between devices with their start and end apart: 4 -> 0, of which waited for: 3 -> 0; matrix products, arithmetic and copies ran while one was open for 10% -> 0% of each run, Pallas kernels for 0% -> 0%
where the time goes in v1:
time: 153 us; the launch traced here: 152 us
  Pallas kernels  114 us (75%)
  local copies, waits for them, and re-layouts  27.5 us (18%)
  matrix products  6.45 us (4%)
  other arithmetic  3.3 us (2%)
    pallas_call x1, Pallas kernels, per_device(): pl.pallas_call(functools.partial(kernel, n, tp, heads), out_shape=(jax.Sh...  114 us
    unnamed x14, local copies, waits for them, and re-layouts  25.4 us
    dot_general x2, matrix products, per_device(): jnp.dot(fall[:, m * rank:(m + 1) * rank], block, preferred_element_type=j...  4.62 us

profile of v1, /device:TPU:0, one launch (start us, length us, event | category | flops | bytes accessed | tf_op | source)
XLA Modules:
  0.0 152.3 jit_solution(4474155648387334907)
XLA Ops:
  0.6 1.6 %convert_element_type.15 = bf16[256,2,512]{2,1,0:T(2,128)(2,1)S(1)} convert(f32[256,2,512]{2,1,0:T(2,128)} %param.19) | non-fusion elementwise | flops 262144 | bytes 1572864 | tf_op jit(solution)/shard_map/convert_element_type | solution.py:274
  2.2 0.9 copy.26
  3.1 1.7 %copy.25 = bf16[32,8,2,256]{3,1,2,0:T(8,128)(2,1)} copy(bf16[32,8,2,256]{3,2,1,0:T(2,128)(2,1)} %bitcast.35) | data formatting | bytes 524288
  4.8 1.6 %copy.32 = f32[32,2,512]{2,0,1:T(8,128)} copy(f32[32,2,512]{2,1,0:T(2,128)} %param.18) | data formatting | bytes 262144 | tf_op args[8]
  6.4 114.2 %shard_map.121 = (bf16[2048,512]{1,0:T(8,128)(2,1)}, bf16[2048,1024]{1,0:T(8,128)(2,1)}, bf16[8,2,32,512]{3,2,1,0:T(8,128)(2,1)}, f32[2,32,512]{2,1,0:T(8,128)}, f32[2,128]{1,0:T(2,128)}) custom-call(bf16[384,2048]{1,0:T(8,128)(2,1)} %x_ref.1, bf16[384,512]{1,0:T(8,128)(2,1)} %q_ref.1, bf16[384,512]{1,0:T(8,128)(2,1)} %k_ref.1, bf16[384,512]{1,0:T(8,128)(2,1)} %v_ref.1, ...), custom_call_target="tpu_custom_call" | custom-call | tf_op jit(solution)/shard_map/pallas_call | solution.py:276
  120.6 0.0 copy-start.2
  120.6 0.0 copy-start.3
  120.6 1.2 fusion.6
  121.9 1.3 rsqrt_multiply_fusion
  123.1 0.5 fusion.8
  123.6 3.3 %fusion = bf16[2048,1,512]{2,0,1:T(8,128)(2,1)S(1)} fusion(bf16[256,512]{1,0:T(8,128)(2,1)S(1)} %bitcast.41, f32[]{:T(128)} %bitcast.4, bf16[2048,1024]{1,0:T(8,128)(2,1)} %get-tuple-element.11, bf16[2048,512]{1,0:T(8,128)(2,1)} %get-tuple-element.12), kind=kOutput, calls=%fused_computation.3 | convolution fusion | flops 541065216 | bytes 5505536 | tf_op jit(solution)/shard_map/dot_general | solution.py:310
  126.9 0.0 copy-done.2
  126.9 0.0 copy-done.3
  126.9 1.3 fusion.1
  128.3 0.4 pad_maximum_fusion
  128.7 0.0 copy-start
  128.7 19.2 %copy.22 = bf16[2048,2,512]{2,1,0:T(2,128)(2,1)} copy(bf16[2048,2,512]{2,0,1:T(8,128)(2,1)S(1)} %pad_maximum_fusion) | data formatting | bytes 8388608
  147.9 0.4 fusion.7
  148.3 0.9 fusion.3
  149.2 0.9 fusion.2
  150.1 0.1 pad_maximum_fusion.1
  150.2 1.3 copy.20
  151.5 0.0 copy-done.1
  151.5 0.8 copy.21
  (2 shorter events, 0.0 us)
Async XLA Ops:
  120.6 6.3 %copy-start.2 = (bf16[2048,1024]{1,0:T(8,128)(2,1)S(1)}, bf16[2048,1024]{1,0:T(8,128)(2,1)}, u32[]{:S(2)}) copy-start(bf16[2048,1024]{1,0:T(8,128)(2,1)} %get-tuple-element.11) | copy-start | bytes 12582916
  120.6 6.3 %copy-start.3 = (bf16[2048,512]{1,0:T(8,128)(2,1)S(1)}, bf16[2048,512]{1,0:T(8,128)(2,1)}, u32[]{:S(2)}) copy-start(bf16[2048,512]{1,0:T(8,128)(2,1)} %get-tuple-element.12) | copy-start | bytes 6291460
  128.7 19.2 %copy-start = (bf16[256,2,256]{2,1,0:T(2,128)(2,1)S(1)}, bf16[256,2,256]{2,1,0:T(2,128)(2,1)}, u32[]{:S(2)}) copy-start(bf16[256,2,256]{2,1,0:T(2,128)(2,1)} %param.17) | copy-start | bytes 786436
  147.9 3.6 %copy-start.1 = (f32[2,32,512]{2,1,0:T(8,128)S(1)}, f32[2,32,512]{2,1,0:T(8,128)}, u32[]{:S(2)}) copy-start(f32[2,32,512]{2,1,0:T(8,128)} %get-tuple-element.10) | copy-start | bytes 393220

commit v2 on v1

--- a/solution.py
+++ b/solution.py
@@ -11,12 +11,13 @@
 BETA = 0.9
 RATE_BASE = 0.5
 MESH = pl.DeviceIdType.MESH
+LANES = 128
 
 
 class Gather:
-    def __init__(self, n, own, slot, send, recv):
+    def __init__(self, n, slot, send, recv):
         me = lax.axis_index("fs")
-        self.own, self.slot, self.send, self.recv = own, slot, send, recv
+        self.slot, self.send, self.recv = slot, send, recv
         self.n, self.me, self.places = n, me, n // 2
         self.place, self.parity = me // 2, me % 2
         self.partner = me + 1 - 2 * self.parity
@@ -28,11 +29,10 @@
             cond = jnp.logical_and(cond, self.place > 0)
         elif way == 1:
             cond = jnp.logical_and(cond, self.place < self.places - 1)
-        mine = index is self.me
 
         def make():
             return pltpu.make_async_remote_copy(
-                src_ref=self.own(half) if mine else self.slot(index, half),
+                src_ref=self.slot(index, half),
                 dst_ref=self.slot(index, half),
                 send_sem=self.send.at[index, half, way],
                 recv_sem=self.recv.at[index, half],
@@ -95,6 +95,10 @@
             @pl.when(cond)
             def _(make=make):
                 make().wait_send()
+
+
+def split(ref, t, tiles, count):
+    return ref[pl.ds(t % tiles * 2 + t // tiles, count, stride=2 * tiles), :]
 
 
 def head_step(head, q_ref, k_ref, v_ref, c_ref, mix_ref, gain_ref, dq_ref, dv_ref):
@@ -142,12 +146,24 @@
 def kernel(
     n, tp, heads,
     x_ref, q_ref, k_ref, v_ref, c_ref, mix_ref, gain_ref, f_ref, mom_ref, w_ref,
-    fall, wall, nmall, nm_ref, tot_ref,
-    dq, dv, psend, precv, sums,
+    fall, wall, nmall, nm_ref, tot_ref, fown,
+    fwide, dq, dv, psend, precv, sums,
     f_send, f_recv, w_send, w_recv, n_send, n_recv, p_send, p_recv, t_send, t_recv,
 ):
     me = lax.axis_index("fs")
     mt = lax.axis_index("tp")
+    deep = fown.shape[0]
+    part = deep // 2
+    rank = fown.shape[1] // 2
+    rank_here = rank // n
+    cols = dq.shape[1]
+    tiles_f, tiles_w = rank // LANES, cols // LANES
+    here = pl.ds(pl.multiple_of(me * deep, deep), deep)
+    fwide[...] = f_ref[...].astype(jnp.float32)
+    for t in range(2 * tiles_f):
+        block = split(fwide, t, tiles_f, deep).astype(jnp.bfloat16)
+        fown[:, t * LANES : (t + 1) * LANES] = block
+        fall[here, t * LANES : (t + 1) * LANES] = block
     barrier = pltpu.get_barrier_semaphore()
     for hop in range(1, n):
         pl.semaphore_signal(barrier, inc=1, device_id={"fs": (me + hop) % n}, device_id_type=MESH)
@@ -155,30 +171,19 @@
         pl.semaphore_signal(barrier, inc=1, device_id={"tp": (mt + hop) % tp}, device_id_type=MESH)
     pl.semaphore_wait(barrier, n - 1 + tp - 1)
 
-    deep = f_ref.shape[0]
-    part = deep // 2
-    rank = f_ref.shape[1] // 2
-    rank_here = rank // n
-
     def rows(ref):
         def slot(index, half):
             return ref.at[pl.ds(pl.multiple_of(index * deep + half * part, part), part)]
 
         return slot
 
-    def own(ref):
-        return lambda half: ref.at[pl.ds(half * part, part)]
-
-    gather_f = Gather(n, own(f_ref), rows(fall), f_send, f_recv)
-    gather_w = Gather(n, own(w_ref), rows(wall), w_send, w_recv)
-    gather_n = Gather(
-        n, lambda half: nmall.at[me, half], lambda i, half: nmall.at[i, half], n_send, n_recv
-    )
+    gather_f = Gather(n, rows(fall), f_send, f_recv)
+    gather_w = Gather(n, rows(wall), w_send, w_recv)
+    gather_n = Gather(n, lambda i, half: nmall.at[i, half], n_send, n_recv)
     gather_f.begin()
+    for t in range(2 * tiles_w):
+        wall[here, t * LANES : (t + 1) * LANES] = split(w_ref, t, tiles_w, deep).astype(jnp.bfloat16)
     gather_w.begin()
-    here = pl.ds(pl.multiple_of(me * deep, deep), deep)
-    fall[here, :] = f_ref[...]
-    wall[here, :] = w_ref[...]
     gather_f.turn()
     done = 1
     for head in range(heads):
@@ -221,9 +226,12 @@
         p_copy(hop).wait_recv()
         total += precv[hop].astype(jnp.float32)
     length = x_ref.shape[0]
-    moments = BETA * mom_ref[...] + total * (length * n) ** (-0.5)
-    nm_ref[...] = moments
-    nmall[me] = moments.astype(nmall.dtype)
+    for t in range(2 * tiles_w):
+        m, lanes = t // tiles_w, slice(t % tiles_w * LANES, (t % tiles_w + 1) * LANES)
+        moments = BETA * split(mom_ref, t, tiles_w, rank_here)
+        moments += total[m, :, lanes] * (length * n) ** (-0.5)
+        nm_ref[m, :, lanes] = moments
+        nmall[me, m, :, lanes] = moments.astype(nmall.dtype)
     gather_n.begin()
     gather_w.step(n // 2 - 1)
     gather_n.turn()
@@ -260,6 +268,52 @@
         gather.finish_send()
 
 
+def finish(entries, fall, wall, nmall, nm_ref, tot_ref, fown, step, nm_out, copies, wide):
+    _, _, rank_here, cols = nmall.shape
+    rank = fall.shape[1] // 2
+    tiles = cols // LANES
+    rate = RATE_BASE / jnp.sqrt(1.0 + tot_ref[...] / entries)
+
+    def lows(rows, m):
+        block = nmall[:, m].reshape(rank, cols).astype(jnp.bfloat16)
+        return jnp.dot(
+            rows[:, m * rank : (m + 1) * rank], block, preferred_element_type=jnp.float32
+        )
+
+    count = fall.shape[0]
+    for m in range(2):
+        low = lows(fall, m)
+        for t in range(tiles):
+            lanes = slice(t * LANES, (t + 1) * LANES)
+            old = wall[:, m * cols + t * LANES : m * cols + (t + 1) * LANES].astype(jnp.float32)
+            wide[pl.ds(2 * t + m, count, stride=2 * tiles), :] = (
+                old - low[:, lanes] * rate[m : m + 1]
+            )
+    copies[...] = wide[...].astype(jnp.bfloat16)
+
+    @pl.when(pl.program_id(0) == 0)
+    def _():
+        for m in range(2):
+            low = lows(fown, m)
+            for t in range(tiles):
+                lanes = slice(t * LANES, (t + 1) * LANES)
+                step[pl.ds(2 * t + m, fown.shape[0], stride=2 * tiles), :] = (
+                    low[:, lanes] * rate[m : m + 1]
+                )
+                nm_out[pl.ds(2 * t + m, rank_here, stride=2 * tiles), :] = nm_ref[m, :, lanes]
+
+
+def to_rows(array):
+    rows, maps, cols = array.shape
+    return array.reshape(rows, maps, cols // LANES, LANES).transpose(0, 2, 1, 3).reshape(-1, LANES)
+
+
+def from_rows(array, rows):
+    return (
+        array.reshape(rows, -1, 2, LANES).transpose(0, 2, 1, 3).reshape(rows, 2, -1)
+    )
+
+
 def per_device(
     n, tp, inputs, queries, keys, values, head_cot, mixing, head_gain, factors, moments, weights
 ):
@@ -270,26 +324,25 @@
     wire = jnp.bfloat16 if rank_here % 16 == 0 else jnp.float32
     vmem = pl.BlockSpec(memory_space=pltpu.VMEM)
     dma = pltpu.SemaphoreType.DMA
-    f_flat = factors.reshape(deep, 2 * rank)
-    w_flat = weights.astype(jnp.bfloat16).reshape(deep, 2 * cols)
-    mom = moments.transpose(1, 0, 2)
-    fall, wall, nmall, nm, totals = pl.pallas_call(
+    held = pl.pallas_call(
         functools.partial(kernel, n, tp, heads),
         out_shape=(
             jax.ShapeDtypeStruct((depth, 2 * rank), jnp.bfloat16),
             jax.ShapeDtypeStruct((depth, 2 * cols), jnp.bfloat16),
             jax.ShapeDtypeStruct((n, 2, rank_here, cols), wire),
             jax.ShapeDtypeStruct((2, rank_here, cols), jnp.float32),
-            jax.ShapeDtypeStruct((2, 128), jnp.float32),
+            jax.ShapeDtypeStruct((2, LANES), jnp.float32),
+            jax.ShapeDtypeStruct((deep, 2 * rank), jnp.bfloat16),
         ),
         in_specs=[vmem] * 5 + [pl.BlockSpec(memory_space=pltpu.SMEM)] + [vmem] * 4,
-        out_specs=(vmem,) * 5,
+        out_specs=(vmem,) * 6,
         scratch_shapes=[
+            pltpu.VMEM((deep * 2 * rank // LANES, LANES), jnp.float32),
             pltpu.VMEM((length, cols), jnp.bfloat16),
             pltpu.VMEM((length, cols), jnp.bfloat16),
             pltpu.VMEM((n, 2, rank_here, cols), wire),
             pltpu.VMEM((n, 2, rank_here, cols), wire),
-            pltpu.VMEM((tp, 2, 128), jnp.float32),
+            pltpu.VMEM((tp, 2, LANES), jnp.float32),
             dma((n, 2, 3)), dma((n, 2)),
             dma((n, 2, 3)), dma((n, 2)),
             dma((n, 2, 3)), dma((n, 2)),
@@ -299,23 +352,40 @@
         compiler_params=pltpu.CompilerParams(
             collective_id=0, has_side_effects=True, vmem_limit_bytes=56 * 1024 * 1024
         ),
-    )(inputs, queries, keys, values, head_cot, mixing, head_gain[None, :], f_flat, mom, w_flat)
-    rate = RATE_BASE / jnp.sqrt(1.0 + totals[:, 0] / (rank * cols * tp))
-    steps, copies = [], []
-    for m in range(2):
-        block = nmall[:, m].reshape(rank, cols).astype(jnp.bfloat16)
-        steps.append(
-            jnp.dot(factors[:, m], block, preferred_element_type=jnp.float32) * rate[m]
-        )
-        low = jnp.dot(
-            fall[:, m * rank : (m + 1) * rank], block, preferred_element_type=jnp.float32
-        )
-        copies.append(
-            (wall[:, m * cols : (m + 1) * cols].astype(jnp.float32) - low * rate[m]).astype(
-                jnp.bfloat16
-            )
-        )
-    return jnp.stack(steps, axis=1), nm.transpose(1, 0, 2), jnp.stack(copies, axis=1)
+    )(
+        inputs, queries, keys, values, head_cot, mixing, head_gain[None, :],
+        to_rows(factors), to_rows(moments), to_rows(weights),
+    )
+    block = min(depth, 256)
+    per_row = 2 * cols // LANES
+
+    def whole(shape):
+        return pl.BlockSpec(shape, lambda i: (0,) * len(shape))
+
+    step, new_moments, copies = pl.pallas_call(
+        functools.partial(finish, rank * cols * tp),
+        grid=(depth // block,),
+        out_shape=(
+            jax.ShapeDtypeStruct((deep * per_row, LANES), jnp.float32),
+            jax.ShapeDtypeStruct((rank_here * per_row, LANES), jnp.float32),
+            jax.ShapeDtypeStruct((depth * per_row, LANES), jnp.bfloat16),
+        ),
+        in_specs=[
+            pl.BlockSpec((block, 2 * rank), lambda i: (i, 0)),
+            pl.BlockSpec((block, 2 * cols), lambda i: (i, 0)),
+            whole((n, 2, rank_here, cols)),
+            whole((2, rank_here, cols)),
+            whole((2, LANES)),
+            whole((deep, 2 * rank)),
+        ],
+        out_specs=(
+            whole((deep * per_row, LANES)),
+            whole((rank_here * per_row, LANES)),
+            pl.BlockSpec((block * per_row, LANES), lambda i: (i, 0)),
+        ),
+        scratch_shapes=[pltpu.VMEM((block * per_row, LANES), jnp.float32)],
+    )(*held)
+    return from_rows(step, deep), from_rows(new_moments, rank_here), from_rows(copies, depth)
 
 
 def solution(mesh):

time: 153 us -> 125 us (0.82)
  local copies, waits for them, and re-layouts: 27.5 us -> 0 us
  Pallas kernels: 114 us -> 124 us
  matrix products: 6.45 us -> 0 us
  other arithmetic: 3.3 us -> 0 us
    unnamed x14 -> x0, local copies, waits for them, and re-layouts: 25.4 us -> none
    pallas_call x0 -> x1, Pallas kernels: none -> 9.28 us  [per_device(): pl.pallas_call(functools.partial(finish, rank * cols * tp), grid=(depth /...]
    dot_general x4 -> x0, matrix products: 6.45 us -> none  [the longest x2 4.62 us: per_device(): jnp.dot(fall[:, m * rank:(m + 1) * rank], block, preferred_element_type=j...]
    slice x3 -> x0, local copies, waits for them, and re-layouts: 2.11 us -> none  [the longest x1 1.22 us: per_device(): block = nmall[:, m].reshape(rank, cols).astype(jnp.bfloat16)]
    convert_element_type x1 -> x0, other arithmetic: 1.59 us -> none  [per_device(): w_flat = weights.astype(jnp.bfloat16).reshape(deep, 2 * cols)]
where the time goes in v2:
time: 125 us
  Pallas kernels  124 us (99%)
    pallas_call x1, Pallas kernels, per_device(): pl.pallas_call(functools.partial(kernel, n, tp, heads), out_shape=(jax.Sh...  115 us
    pallas_call x1, Pallas kernels, per_device(): pl.pallas_call(functools.partial(finish, rank * cols * tp), grid=(depth /...  9.28 us

profile of v2, /device:TPU:0, one launch (start us, length us, event | category | flops | bytes accessed | tf_op | source)
XLA Modules:
  0.0 124.5 jit_solution(3110253075364432380)
XLA Ops:
  0.6 114.6 %shard_map.121 = (bf16[2048,512]{1,0:T(8,128)(2,1)}, bf16[2048,1024]{1,0:T(8,128)(2,1)}, bf16[8,2,32,512]{3,2,1,0:T(8,128)(2,1)}, f32[2,32,512]{2,1,0:T(8,128)},...) custom-call(bf16[384,2048]{1,0:T(8,128)(2,1)} %x_ref.1, bf16[384,512]{1,0:T(8,128)(2,1)} %q_ref.1, bf16[384,512]{1,0:T(8,128)(2,1)} %k_ref.1, ...), custom_call_target="tpu_custom_call" | custom-call | tf_op jit(solution)/shard_map/pallas_call | solution.py:327
  115.3 9.3 %shard_map.122 = (f32[2048,128]{1,0:T(8,128)}, f32[256,128]{1,0:T(8,128)}, bf16[16384,128]{1,0:T(8,128)(2,1)}) custom-call(bf16[2048,512]{1,0:T(8,128)(2,1)} %get-tuple-element.12.fall, bf16[2048,1024]{1,0:T(8,128)(2,1)} %get-tuple-element.13.wall, bf16[8,2,32,512]{3,2,1,0:T(8,128)(2,1)} %get-tuple-element.14.nmall, f32[2,32,512]{2,1,0:T(8,128)} %get-tuple-element.15.nm_ref, ...), custom_call_target="tpu_custom_call" | custom-call | tf_op jit(solution)/shard_map/pallas_call | solution.py:365

commit v3 on v2

--- a/solution.py
+++ b/solution.py
@@ -15,9 +15,9 @@
 
 
 class Gather:
-    def __init__(self, n, slot, send, recv):
+    def __init__(self, n, slot, send, recv, hook=None):
         me = lax.axis_index("fs")
-        self.slot, self.send, self.recv = slot, send, recv
+        self.slot, self.send, self.recv, self.hook = slot, send, recv, hook
         self.n, self.me, self.places = n, me, n // 2
         self.place, self.parity = me // 2, me % 2
         self.partner = me + 1 - 2 * self.parity
@@ -57,6 +57,8 @@
                 device_id={"fs": self.partner},
                 device_id_type=MESH,
             ).wait_recv()
+            if self.hook is not None:
+                self.hook(index, half)
 
     def begin(self):
         true = self.me >= 0
@@ -148,7 +150,7 @@
     x_ref, q_ref, k_ref, v_ref, c_ref, mix_ref, gain_ref, f_ref, mom_ref, w_ref,
     fall, wall, nmall, nm_ref, tot_ref, fown,
     fwide, dq, dv, psend, precv, sums,
-    f_send, f_recv, w_send, w_recv, n_send, n_recv, p_send, p_recv, t_send, t_recv,
+    f_send, f_recv, s_send, s_recv, w_send, w_recv, n_send, n_recv, p_send, p_recv, t_send, t_recv,
 ):
     me = lax.axis_index("fs")
     mt = lax.axis_index("tp")
@@ -177,7 +179,51 @@
 
         return slot
 
-    gather_f = Gather(n, rows(fall), f_send, f_recv)
+    quarter = 2 * rank // tp
+    far, near = (mt + 2) % tp, mt + 1 - 2 * (mt % 2)
+
+    def quarters(index, half, which):
+        return fall.at[
+            pl.ds(pl.multiple_of(index * deep + half * part, part), part),
+            pl.ds(pl.multiple_of(which * quarter, quarter), quarter),
+        ]
+
+    def spread(index, half, which, target, way):
+        return pltpu.make_async_remote_copy(
+            src_ref=quarters(index, half, which),
+            dst_ref=quarters(index, half, which),
+            send_sem=s_send.at[index, half, way],
+            recv_sem=s_recv.at[index, half, way],
+            device_id={"tp": target},
+            device_id_type=MESH,
+        )
+
+    def hook(index, half):
+        spread(index, half, mt, far, 0).start()
+        spread(index, half, mt, near, 1).start()
+
+    def spread_all():
+        pieces = [((me + hop) % n, half) for hop in range(1, n) for half in (0, 1)]
+        for index, half in pieces:
+            spread(index, half, far, far, 0).wait_recv()
+            spread(index, half, far, near, 2).start()
+        for index, half in pieces:
+            spread(index, half, near, near, 1).wait_recv()
+            spread(index, half, (near + 2) % tp, near, 2).wait_recv()
+
+    def spread_sent():
+        for hop in range(1, n):
+            for half in (0, 1):
+                index = (me + hop) % n
+                spread(index, half, mt, far, 0).wait_send()
+                spread(index, half, mt, near, 1).wait_send()
+                spread(index, half, far, near, 2).wait_send()
+
+    if tp == 4 and quarter % LANES == 0:
+        gather_f = Gather(n, lambda i, half: quarters(i, half, mt), f_send, f_recv, hook)
+    else:
+        spread_all = spread_sent = lambda: None
+        gather_f = Gather(n, rows(fall), f_send, f_recv)
     gather_w = Gather(n, rows(wall), w_send, w_recv)
     gather_n = Gather(n, lambda i, half: nmall.at[i, half], n_send, n_recv)
     gather_f.begin()
@@ -195,6 +241,7 @@
         gather_f.step(s)
     gather_w.turn()
     gather_f.finish_recv()
+    spread_all()
     gather_w.step(1)
     for m, cot in enumerate((dq, dv)):
         reduced = jnp.dot(
@@ -264,6 +311,7 @@
         t_copy(hop).wait_send()
     for hop in range(1, n):
         p_copy(hop).wait_send()
+    spread_sent()
     for gather in (gather_f, gather_w, gather_n):
         gather.finish_send()
 
@@ -343,7 +391,7 @@
             pltpu.VMEM((n, 2, rank_here, cols), wire),
             pltpu.VMEM((n, 2, rank_here, cols), wire),
             pltpu.VMEM((tp, 2, LANES), jnp.float32),
-            dma((n, 2, 3)), dma((n, 2)),
+            dma((n, 2, 3)), dma((n, 2)), dma((n, 2, 3)), dma((n, 2, 3)),
             dma((n, 2, 3)), dma((n, 2)),
             dma((n, 2, 3)), dma((n, 2)),
             dma((n,)), dma((n,)),

time: 125 us -> 109 us (0.87)
  Pallas kernels: 124 us -> 108 us
    pallas_call x1, Pallas kernels: 115 us -> 98.7 us  [per_device(): pl.pallas_call(functools.partial(kernel, n, tp, heads), out_shape=(jax.Sh...]
where the time goes in v3:
time: 109 us
  Pallas kernels  108 us (99%)
    pallas_call x1, Pallas kernels, per_device(): pl.pallas_call(functools.partial(kernel, n, tp, heads), out_shape=(jax.Sh...  98.7 us
    pallas_call x1, Pallas kernels, per_device(): pl.pallas_call(functools.partial(finish, rank * cols * tp), grid=(depth /...  9.28 us

profile of v3, /device:TPU:0, one launch (start us, length us, event | category | flops | bytes accessed | tf_op | source)
XLA Modules:
  0.0 108.6 jit_solution(10767751866633389668)
XLA Ops:
  0.6 98.7 %shard_map.121 = (bf16[2048,512]{1,0:T(8,128)(2,1)}, bf16[2048,1024]{1,0:T(8,128)(2,1)}, bf16[8,2,32,512]{3,2,1,0:T(8,128)(2,1)}, f32[2,32,512]{2,1,0:T(8,128)},...) custom-call(bf16[384,2048]{1,0:T(8,128)(2,1)} %x_ref.1, bf16[384,512]{1,0:T(8,128)(2,1)} %q_ref.1, bf16[384,512]{1,0:T(8,128)(2,1)} %k_ref.1, ...), custom_call_target="tpu_custom_call" | custom-call | tf_op jit(solution)/shard_map/pallas_call | solution.py:375
  99.3 9.3 %shard_map.122 = (f32[2048,128]{1,0:T(8,128)}, f32[256,128]{1,0:T(8,128)}, bf16[16384,128]{1,0:T(8,128)(2,1)}) custom-call(bf16[2048,512]{1,0:T(8,128)(2,1)} %get-tuple-element.12.fall, bf16[2048,1024]{1,0:T(8,128)(2,1)} %get-tuple-element.13.wall, bf16[8,2,32,512]{3,2,1,0:T(8,128)(2,1)} %get-tuple-element.14.nmall, f32[2,32,512]{2,1,0:T(8,128)} %get-tuple-element.15.nm_ref, ...), custom_call_target="tpu_custom_call" | custom-call | tf_op jit(solution)/shard_map/pallas_call | solution.py:413

commit v4 on v3

--- a/solution.py
+++ b/solution.py
@@ -156,6 +156,7 @@
     mt = lax.axis_index("tp")
     deep = fown.shape[0]
     part = deep // 2
+    cut = max(16, deep // 64 * 16)
     rank = fown.shape[1] // 2
     rank_here = rank // n
     cols = dq.shape[1]
@@ -175,7 +176,8 @@
 
     def rows(ref):
         def slot(index, half):
-            return ref.at[pl.ds(pl.multiple_of(index * deep + half * part, part), part)]
+            start, size = (cut, deep - cut) if half else (0, cut)
+            return ref.at[pl.ds(pl.multiple_of(index * deep + start, 16), size)]
 
         return slot
 

time: 109 us -> 103 us (0.945)
  Pallas kernels: 108 us -> 102 us
    pallas_call x1, Pallas kernels: 98.7 us -> 93 us  [per_device(): pl.pallas_call(functools.partial(kernel, n, tp, heads), out_shape=(jax.Sh...]
where the time goes in v4:
time: 103 us
  Pallas kernels  102 us (99%)
    pallas_call x1, Pallas kernels, per_device(): pl.pallas_call(functools.partial(kernel, n, tp, heads), out_shape=(jax.Sh...  93 us
    pallas_call x1, Pallas kernels, per_device(): pl.pallas_call(functools.partial(finish, rank * cols * tp), grid=(depth /...  9.28 us

profile of v4, /device:TPU:0, one launch (start us, length us, event | category | flops | bytes accessed | tf_op | source)
XLA Modules:
  0.0 102.9 jit_solution(9811179509677707119)
XLA Ops:
  0.6 93.0 %shard_map.121 = (bf16[2048,512]{1,0:T(8,128)(2,1)}, bf16[2048,1024]{1,0:T(8,128)(2,1)}, bf16[8,2,32,512]{3,2,1,0:T(8,128)(2,1)}, f32[2,32,512]{2,1,0:T(8,128)},...) custom-call(bf16[384,2048]{1,0:T(8,128)(2,1)} %x_ref.1, bf16[384,512]{1,0:T(8,128)(2,1)} %q_ref.1, bf16[384,512]{1,0:T(8,128)(2,1)} %k_ref.1, ...), custom_call_target="tpu_custom_call" | custom-call | tf_op jit(solution)/shard_map/pallas_call | solution.py:377
  93.6 9.3 %shard_map.122 = (f32[2048,128]{1,0:T(8,128)}, f32[256,128]{1,0:T(8,128)}, bf16[16384,128]{1,0:T(8,128)(2,1)}) custom-call(bf16[2048,512]{1,0:T(8,128)(2,1)} %get-tuple-element.12.fall, bf16[2048,1024]{1,0:T(8,128)(2,1)} %get-tuple-element.13.wall, bf16[8,2,32,512]{3,2,1,0:T(8,128)(2,1)} %get-tuple-element.14.nmall, f32[2,32,512]{2,1,0:T(8,128)} %get-tuple-element.15.nm_ref, ...), custom_call_target="tpu_custom_call" | custom-call | tf_op jit(solution)/shard_map/pallas_call | solution.py:415
